TPU v7x, 512 devices: a whole 4x4x16 slice. The times are simulated.
512 devices in a mesh: sp: 32 (over z, core), tp: 16 (over y, x).
Axes of the slice: x: 4, y: 4, z: 16, core: 2. Of those that a mesh axis runs over, the one named last changes fastest.
Arguments:
- layer_input: bfloat16 [32768, 4096], P('sp', 'tp'), may hold values from -6 to 6
- key_weight: bfloat16 [4096, 4096], P(None, 'tp'), may hold values from -0.09375 to 0.09375
- value_weight: bfloat16 [4096, 4096], P(None, 'tp'), may hold values from -0.09375 to 0.09375
- decay_exponent: float32 [32], P('tp'), may hold values from -0.077 to -4.2114258e-05, as said below
- query_new: bfloat16 [2, 4096], P(None, 'tp'), may hold values from -6 to 6
- key_new: bfloat16 [2, 4096], P(None, 'tp'), may hold values from -6 to 6
- value_new: bfloat16 [2, 4096], P(None, 'tp'), may hold values from -6 to 6
- norm_gain: float32 [4096], P('tp'), may hold values from 0.1 to 1.9
Outputs:
- state_cache: bfloat16 [2, 32, 128, 128], P(None, 'tp', 'sp')
- first_read: bfloat16 [2, 4096], P(None, 'tp')
Inputs may be any that keep to these rules, and one draw needn't show every extreme that they name: decay_exponent is negative.
All inputs are finite; a program needn't handle non-finite values.
Results may differ from a plain program's by a relative error of at most 0.011.
Values may be sent and summed in bfloat16 or wider, within the bound.
A program may use at most 64 MiB of HBM per device.

v0:
```python
import jax
import jax.numpy as jnp
from jax import lax
from jax.sharding import PartitionSpec as P

SEQS = 2


def in_blocks(x, dim, peers):
    before, after = (x.shape[:dim], x.shape[dim + 1 :])
    return jnp.moveaxis(x.reshape(*before, peers, -1, *after), dim, 0)


def sent_and_summed(x, axis, dim):
    tiles = in_blocks(x, dim, lax.axis_size(axis))
    arrived = lax.all_to_all(tiles, axis, split_axis=0, concat_axis=0, tiled=True)
    return arrived.astype(jnp.float32).sum(axis=0)


def copy_for_each(x, axis):
    copies = jnp.broadcast_to(x, (lax.axis_size(axis), *x.shape))
    return lax.all_to_all(copies, axis, split_axis=0, concat_axis=0, tiled=True)


def of_everyone(x, axis):
    return copy_for_each(x, axis).sum(axis=0)


def rotate(projected, position):
    half_width = projected.shape[-1] // 2
    inverse = 1.0 / 10000.0 ** jnp.linspace(0.0, 1.0, half_width, dtype=jnp.float32)
    angle = position[:, None] * inverse[None, :]
    cosine = jnp.cos(angle)[:, None, :]
    sine = jnp.sin(angle)[:, None, :]
    first = projected[..., :half_width]
    second = projected[..., half_width:]
    return jnp.concatenate(
        [first * cosine - second * sine, first * sine + second * cosine], axis=-1
    )


def on_device(
    layer_input, key_weight, value_weight, decay_exponent, query_new, key_new, value_new, norm_gain
):
    tok_count = layer_input.shape[0]
    head_local = decay_exponent.shape[0]
    key_width = key_weight.shape[1] // head_local
    value_width = value_weight.shape[1] // head_local
    seq_span = lax.axis_size("sp") // SEQS
    seq_length = tok_count * seq_span
    sp_place = lax.axis_index("sp")
    feature_block = lax.all_gather(layer_input, "tp", axis=1, tiled=True)
    key_proj = jnp.dot(feature_block, key_weight, preferred_element_type=jnp.float32)
    value_proj = jnp.dot(feature_block, value_weight, preferred_element_type=jnp.float32)
    position = (sp_place % seq_span * tok_count + jnp.arange(tok_count, dtype=jnp.int32)).astype(
        jnp.float32
    )
    keys = (
        rotate(key_proj.reshape(tok_count, head_local, key_width), position) * key_width ** (-0.5)
    ).astype(jnp.bfloat16)
    values = value_proj.astype(jnp.bfloat16).reshape(tok_count, head_local, value_width)
    distance = seq_length - 1.0 - position
    weighting = jnp.exp(decay_exponent[None, :] * distance[:, None])
    weighted = (keys.astype(jnp.float32) * weighting[:, :, None]).astype(jnp.bfloat16)
    local_state = jnp.einsum("thd,the->hde", weighted, values, preferred_element_type=jnp.float32)
    member = (jnp.arange(SEQS, dtype=jnp.int32) == sp_place // seq_span).astype(jnp.float32)
    state_terms = member[:, None, None, None] * local_state[None]
    final_rows = sent_and_summed(state_terms.astype(jnp.bfloat16), "sp", 2)
    state_cache = final_rows.astype(jnp.bfloat16)
    queries = query_new.astype(jnp.float32).reshape(SEQS, head_local, key_width)
    partial_read = jnp.einsum(
        "shd,shde->she", queries, state_terms, precision=lax.Precision.HIGHEST
    )
    carried = of_everyone(partial_read, "sp")
    keys_next = key_new.astype(jnp.float32).reshape(SEQS, head_local, key_width)
    values_next = value_new.astype(jnp.float32).reshape(SEQS, head_local, value_width)
    own_term = jnp.sum(queries * keys_next, axis=2)[:, :, None] * values_next
    mixed = jnp.exp(decay_exponent)[None, :, None] * carried + own_term
    normed = mixed * lax.rsqrt(jnp.mean(mixed * mixed, axis=2, keepdims=True) + 1e-06)
    normed = normed * norm_gain.reshape(head_local, value_width)[None, :, :]
    return (state_cache, normed.reshape(SEQS, head_local * value_width).astype(jnp.bfloat16))


def solution(mesh):
    in_specs = (
        P("sp", "tp"),
        P(None, "tp"),
        P(None, "tp"),
        P("tp"),
        P(None, "tp"),
        P(None, "tp"),
        P(None, "tp"),
        P("tp"),
    )
    out_specs = (P(None, "tp", "sp", None), P(None, "tp"))
    return jax.shard_map(
        on_device, mesh=mesh, in_specs=in_specs, out_specs=out_specs, check_vma=False
    )
```

profile of v0, /device:TPU:1, one launch (start us, length us, event | category | flops | bytes accessed | tf_op | source)
XLA Modules:
  0.0 174.9 jit_solution(16979299565072083331)
XLA Ops:
  7.2 0.0 copy-start
  7.2 0.0 all-gather.2.cloned.1.call-start
  7.2 0.7 all-gather.2.cloned.1.call-update
  7.9 0.7 reshape.155
  8.6 0.7 exp.11
  9.3 0.1 fusion.12
  9.4 0.7 convert_multiply_fusion
  10.1 0.7 multiply_exponential_fusion
  10.8 1.0 multiply_cosine_fusion
  11.8 95.6 %all-gather.2.cloned.1.call-done = bf16[1024,4096]{1,0:T(8,128)(2,1)} async-done(((bf16[1024,256]{1,0:T(8,128)(2,1)}), bf16[1024,4096]{1,0:T(8,128)(2,1)}) %all-gather.2.cloned.1.call-update) | async-done | bytes 8388624 | tf_op jit(solution)/shard_map/all_gather | solution.py:52
  107.5 0.0 copy-done
  107.5 0.0 copy-start.3
  107.5 5.9 %fusion.15 = f32[1024,256]{0,1:T(8,128)S(1)} fusion(bf16[1024,4096]{1,0:T(8,128)(2,1)} %all-gather.2.cloned.1.call-done, bf16[4096,256]{1,0:T(8,128)(2,1)S(1)} %copy-done), kind=kOutput, calls=%fused_computation.37 | convolution fusion | flops 2147483648 | bytes 11534336 | tf_op jit(solution)/shard_map/dot_general | solution.py:53
  113.4 0.0 copy-start.4
  113.4 0.2 multiply_subtract_fusion
  113.5 0.0 copy-done.3
  113.6 1.4 copy-done.4
  115.0 2.4 %convolution_convert_fusion = bf16[1024,256]{0,1:T(8,128)(2,1)S(1)} fusion(bf16[1024,4096]{1,0:T(8,128)(2,1)S(1)} %copy-done.3, bf16[4096,256]{1,0:T(8,128)(2,1)S(1)} %copy-done.4), kind=kOutput, calls=%fused_computation | convolution fusion | flops 2147745792 | bytes 11010048 | tf_op jit(solution)/shard_map/dot_general | solution.py:54
  117.4 0.0 copy-start.1
  117.4 0.0 copy-start.2
  117.4 0.3 fusion.1
  117.7 0.3 fusion.5
  118.0 0.6 broadcast_in_dim.4
  118.7 14.4 %all-to-all-start.1 = ((f32[32,2,2,128]{3,2,1,0:T(2,128)}), f32[32,2,2,128]{3,2,1,0:T(2,128)S(1)}, u32[]{:S(2)}, u32[]{:S(2)}) async-start(f32[32,2,2,128]{3,2,1,0:T(2,128)} %broadcast_in_dim.4), calls=%async_computation.1 | async-start | bytes 131072 | tf_op jit(solution)/shard_map/all_to_all | solution.py:22
  133.1 0.1 broadcast_bitcast_fusion.2
  133.1 0.0 copy-done.1
  133.2 0.1 reduce_sum.44
  133.2 0.8 multiply_convert_fusion.2
  134.0 12.1 %all-to-all-done.1 = f32[32,2,2,128]{3,2,1,0:T(2,128)S(1)} async-done(((f32[32,2,2,128]{3,2,1,0:T(2,128)}), f32[32,2,2,128]{3,2,1,0:T(2,128)S(1)}, u32[]{:S(2)}, u32[]{:S(2)}) %all-to-all-start.1) | async-done | bytes 65568 | tf_op jit(solution)/shard_map/all_to_all | solution.py:22
  146.1 5.1 %all-to-all-start = ((bf16[32,2,2,4,128]{4,3,2,1,0:T(4,128)(2,1)}), bf16[32,2,2,4,128]{4,3,2,1,0:T(4,128)(2,1)S(1)}, u32[]{:S(2)}, u32[]{:S(2)}) async-start(bf16[32,2,2,4,128]{4,3,2,1,0:T(4,128)(2,1)} %multiply_convert_fusion.2), calls=%async_computation | async-start | bytes 262144 | tf_op jit(solution)/shard_map/all_to_all | solution.py:16
  151.2 0.2 broadcast_bitcast_fusion.1
  151.4 0.1 broadcast_bitcast_fusion
  151.5 0.0 copy-done.2
  151.5 0.6 fusion.10
  152.0 15.3 %all-to-all-done = bf16[32,2,2,4,128]{4,3,2,1,0:T(4,128)(2,1)S(1)} async-done(((bf16[32,2,2,4,128]{4,3,2,1,0:T(4,128)(2,1)}), bf16[32,2,2,4,128]{4,3,2,1,0:T(4,128)(2,1)S(1)}, u32[]{:S(2)}, u32[]{:S(2)}) %all-to-all-start) | async-done | bytes 131104 | tf_op jit(solution)/shard_map/all_to_all | solution.py:16
  167.4 0.7 reduce_sum.41
  (8 shorter events, 0.1 us)
Async XLA Ops:
  7.2 100.3 %copy-start = (bf16[4096,256]{1,0:T(8,128)(2,1)S(1)}, bf16[4096,256]{1,0:T(8,128)(2,1)}, u32[]{:S(2)}) copy-start(bf16[4096,256]{1,0:T(8,128)(2,1)} %param.9) | copy-start | bytes 6291460
  7.2 100.3 %all-gather.2.cloned.1.call-start = ((), (), s32[]{:S(2)}) async-start(), calls=%async_computation.2 | async-start | bytes 8912896 | tf_op jit(solution)/shard_map/all_gather | solution.py:52
  107.5 6.1 %copy-start.3 = (bf16[1024,4096]{1,0:T(8,128)(2,1)S(1)}, bf16[1024,4096]{1,0:T(8,128)(2,1)}, u32[]{:S(2)}) copy-start(bf16[1024,4096]{1,0:T(8,128)(2,1)} %all-gather.2.cloned.1.call-done) | copy-start | bytes 25165828
  113.4 1.6 copy-start.4
  117.4 15.8 %copy-start.1 = (bf16[2,256]{1,0:T(2,128)(2,1)S(1)}, bf16[2,256]{1,0:T(2,128)(2,1)}, u32[]{:S(2)}) copy-start(bf16[2,256]{1,0:T(2,128)(2,1)} %param.14) | copy-start | bytes 3076
  117.4 34.1 %copy-start.2 = (f32[256]{0:T(256)S(1)}, f32[256]{0:T(256)}, u32[]{:S(2)}) copy-start(f32[256]{0:T(256)} %param.15) | copy-start | bytes 3076
  118.7 27.4 %all-to-all-start.1 = ((f32[32,2,2,128]{3,2,1,0:T(2,128)}), f32[32,2,2,128]{3,2,1,0:T(2,128)S(1)}, u32[]{:S(2)}, u32[]{:S(2)}) async-start(f32[32,2,2,128]{3,2,1,0:T(2,128)} %broadcast_in_dim.4), calls=%async_computation.1 | async-start | bytes 131072 | tf_op jit(solution)/shard_map/all_to_all | solution.py:22
  146.1 21.3 %all-to-all-start = ((bf16[32,2,2,4,128]{4,3,2,1,0:T(4,128)(2,1)}), bf16[32,2,2,4,128]{4,3,2,1,0:T(4,128)(2,1)S(1)}, u32[]{:S(2)}, u32[]{:S(2)}) async-start(bf16[32,2,2,4,128]{4,3,2,1,0:T(4,128)(2,1)} %multiply_convert_fusion.2), calls=%async_computation | async-start | bytes 262144 | tf_op jit(solution)/shard_map/all_to_all | solution.py:16
Sparse Core Ops, SparseCore 0:
  11.0 96.4 all-gather.1
where the time goes:
time: 175 us
  waiting for transfers between devices  124 us (71%)
  starting transfers between devices  19.5 us (11%)
  between operations  14.2 us (8%)
  matrix products  8.92 us (5%)
  other arithmetic  4.99 us (3%)
  local copies, waits for them, and re-layouts  3.61 us (2%)
    all_gather x1, waiting for transfers between devices, on_device(): feature_block = lax.all_gather(layer_input, 'tp', axis=1, tiled=True)  95.6 us
    all_to_all x1, waiting for transfers between devices, sent_and_summed(): lax.all_to_all(tiles, axis, split_axis=0, concat_axis=0, tiled=True)  15.3 us
    all_to_all x1, starting transfers between devices, copy_for_each(): return lax.all_to_all(copies, axis, split_axis=0, concat_axis=0, tiled=True)  14.4 us
    all_to_all x1, waiting for transfers between devices, copy_for_each(): return lax.all_to_all(copies, axis, split_axis=0, concat_axis=0, tiled=True)  12.1 us
    dot_general x1, matrix products, on_device(): jnp.dot(feature_block, key_weight, preferred_element_type=jnp.float32)  5.9 us
    all_to_all x1, starting transfers between devices, sent_and_summed(): lax.all_to_all(tiles, axis, split_axis=0, concat_axis=0, tiled=True)  5.1 us
  transfers between devices with their start and end apart: 3, of which 3 were waited for; matrix products, arithmetic and copies ran while one was open for 3% of the time, Pallas kernels for 0%

commit v1 on v0

--- a/solution.py
+++ b/solution.py
@@ -49,7 +49,12 @@
     seq_span = lax.axis_size("sp") // SEQS
     seq_length = tok_count * seq_span
     sp_place = lax.axis_index("sp")
-    feature_block = lax.all_gather(layer_input, "tp", axis=1, tiled=True)
+
+    def recast_modes_now(my_tile):
+        out_arr = jnp.concatenate(lax.all_gather(my_tile, axis_name="tp"), axis=1)
+        return out_arr
+
+    feature_block = recast_modes_now(layer_input)
     key_proj = jnp.dot(feature_block, key_weight, preferred_element_type=jnp.float32)
     value_proj = jnp.dot(feature_block, value_weight, preferred_element_type=jnp.float32)
     position = (sp_place % seq_span * tok_count + jnp.arange(tok_count, dtype=jnp.int32)).astype(

time: 175 us -> 201 us (1.15)
  local copies, waits for them, and re-layouts: 3.61 us -> 39.4 us
  waiting for transfers between devices: 124 us -> 114 us
    reshape x0 -> x1, local copies, waits for them, and re-layouts: none -> 13.5 us  [recast_modes_now(): out_arr = jnp.concatenate(lax.all_gather(my_tile, axis_name='tp'), axis=1)]
    all_gather x0 -> x1, local copies, waits for them, and re-layouts: none -> 11.4 us  [recast_modes_now(): out_arr = jnp.concatenate(lax.all_gather(my_tile, axis_name='tp'), axis=1)]
    all_gather x1, waiting for transfers between devices: 95.6 us -> 86.3 us  [recast_modes_now(): out_arr = jnp.concatenate(lax.all_gather(my_tile, axis_name='tp'), axis=1)]
    unnamed x11 -> x12, local copies, waits for them, and re-layouts: 1.51 us -> 8.3 us
    dot_general x0 -> x1, local copies, waits for them, and re-layouts: none -> 4.13 us  [on_device(): jnp.dot(feature_block, key_weight, preferred_element_type=jnp.float32)]
    dot_general x1, matrix products: 5.9 us -> 2.36 us  [on_device(): jnp.dot(feature_block, key_weight, preferred_element_type=jnp.float32)]
    dot_general x1, matrix products: 2.41 us -> 5.9 us  [on_device(): jnp.dot(feature_block, value_weight, preferred_element_type=jnp.float32)]
  transfers between devices with their start and end apart: 3 -> 3, of which waited for: 3 -> 3; matrix products, arithmetic and copies ran while one was open for 3% -> 5% of each run, Pallas kernels for 0% -> 0%
where the time goes in v1:
time: 201 us; the launch traced here: 200 us
  waiting for transfers between devices  114 us (57%)
  local copies, waits for them, and re-layouts  39.4 us (20%)
  starting transfers between devices  18.3 us (9%)
  between operations  14.1 us (7%)
  matrix products  8.88 us (4%)
  other arithmetic  4.99 us (2%)
    all_gather x1, waiting for transfers between devices, recast_modes_now(): out_arr = jnp.concatenate(lax.all_gather(my_tile, axis_name='tp'), axis=1)  86.3 us
    all_to_all x1, waiting for transfers between devices, sent_and_summed(): lax.all_to_all(tiles, axis, split_axis=0, concat_axis=0, tiled=True)  15.3 us
    reshape x1, local copies, waits for them, and re-layouts, recast_modes_now(): out_arr = jnp.concatenate(lax.all_gather(my_tile, axis_name='tp'), axis=1)  13.5 us
    all_to_all x1, starting transfers between devices, copy_for_each(): return lax.all_to_all(copies, axis, split_axis=0, concat_axis=0, tiled=True)  13.2 us
    all_to_all x1, waiting for transfers between devices, copy_for_each(): return lax.all_to_all(copies, axis, split_axis=0, concat_axis=0, tiled=True)  12.1 us
    all_gather x1, local copies, waits for them, and re-layouts, recast_modes_now(): out_arr = jnp.concatenate(lax.all_gather(my_tile, axis_name='tp'), axis=1)  11.4 us
    unnamed x12, local copies, waits for them, and re-layouts  8.3 us
    dot_general x1, matrix products, on_device(): jnp.dot(feature_block, value_weight, preferred_element_type=jnp.float32)  5.9 us
  transfers between devices with their start and end apart: 3, of which 3 were waited for; matrix products, arithmetic and copies ran while one was open for 5% of the time, Pallas kernels for 0%

profile of v1, /device:TPU:1, one launch (start us, length us, event | category | flops | bytes accessed | tf_op | source)
XLA Modules:
  0.0 200.1 jit_solution(17558376233590204284)
XLA Ops:
  7.2 0.0 copy-start
  7.2 0.0 all-gather.3.cloned.1.call-start
  7.2 0.7 all-gather.3.cloned.1.call-update
  7.9 4.1 %copy.27 = bf16[256,4096]{1,0:T(8,128)(2,1)} copy(bf16[256,4096]{0,1:T(8,128)(2,1)} %bitcast.49) | data formatting | bytes 4194304 | tf_op jit(solution)/shard_map/dot_general | solution.py:58
  12.1 0.7 reshape.164
  12.8 0.7 exp.11
  13.4 0.1 fusion.12
  13.5 0.7 convert_multiply_fusion
  14.2 0.7 multiply_exponential_fusion
  15.0 1.0 multiply_cosine_fusion
  16.0 86.3 %all-gather.3.cloned.1.call-done = bf16[16384,256]{1,0:T(8,128)(2,1)} async-done(((bf16[1024,256]{1,0:T(8,128)(2,1)}), bf16[16384,256]{1,0:T(8,128)(2,1)}) %all-gather.3.cloned.1.call-update) | async-done | bytes 8388624 | tf_op jit(solution)/shard_map/all_gather | solution.py:54
  102.3 7.8 %copy.30 = bf16[128,8,16,256]{3,1,2,0:T(8,128)(2,1)} copy(bf16[128,8,16,256]{3,1,0,2:T(8,128)(2,1)} %bitcast.45) | data formatting | bytes 16777216
  110.0 11.4 %copy.41 = bf16[16,1024,256]{2,0,1:T(8,128)(2,1)} copy(bf16[16,1024,256]{2,1,0:T(8,128)(2,1)} %bitcast.46) | data formatting | bytes 16777216 | tf_op jit(solution)/shard_map/all_gather | solution.py:54
  121.4 13.5 %reshape.159 = bf16[1024,4096,1]{1,0,2:T(8,128)(2,1)} reshape(bf16[1024,16,256]{2,1,0:T(8,128)(2,1)} %bitcast.47) | data formatting | bytes 16777216 | tf_op jit(solution)/shard_map/reshape | solution.py:54
  134.9 0.0 copy-done
  134.9 0.0 copy-start.1
  134.9 0.0 copy-start.2
  134.9 5.9 %convolution_convert_fusion = bf16[1024,256]{0,1:T(8,128)(2,1)S(1)} fusion(bf16[1024,4096]{1,0:T(8,128)(2,1)} %bitcast.48, bf16[4096,256]{1,0:T(8,128)(2,1)S(1)} %copy-done), kind=kOutput, calls=%fused_computation | convolution fusion | flops 2147745792 | bytes 11010048 | tf_op jit(solution)/shard_map/dot_general | solution.py:59
  140.8 0.0 copy-done.1
  140.8 0.4 copy-done.2
  141.2 0.0 copy-start.3
  141.2 0.0 copy-start.4
  141.2 2.4 %fusion.15 = f32[1024,2,128]{0,2,1:T(8,128)S(1)} fusion(bf16[1024,4096,1]{1,0,2:T(8,128)(2,1)S(1)} %copy-done.1, bf16[2,128,4096]{2,1,0:T(8,128)(2,1)S(1)} %bitcast.50), kind=kOutput, calls=%fused_computation.38 | convolution fusion | flops 2147483648 | bytes 11534336 | tf_op jit(solution)/shard_map/dot_general | solution.py:58
  143.6 0.2 multiply_subtract_fusion
  143.8 0.3 fusion.1
  144.1 0.3 fusion.5
  144.4 0.6 broadcast_in_dim.4
  145.1 13.2 %all-to-all-start.1 = ((f32[32,2,2,128]{3,2,1,0:T(2,128)}), f32[32,2,2,128]{3,2,1,0:T(2,128)S(1)}, u32[]{:S(2)}, u32[]{:S(2)}) async-start(f32[32,2,2,128]{3,2,1,0:T(2,128)} %broadcast_in_dim.4), calls=%async_computation.1 | async-start | bytes 131072 | tf_op jit(solution)/shard_map/all_to_all | solution.py:22
  158.2 0.1 broadcast_bitcast_fusion.2
  158.3 0.0 copy-done.3
  158.3 0.1 reduce_sum.44
  158.4 0.8 multiply_convert_fusion.2
  159.2 12.1 %all-to-all-done.1 = f32[32,2,2,128]{3,2,1,0:T(2,128)S(1)} async-done(((f32[32,2,2,128]{3,2,1,0:T(2,128)}), f32[32,2,2,128]{3,2,1,0:T(2,128)S(1)}, u32[]{:S(2)}, u32[]{:S(2)}) %all-to-all-start.1) | async-done | bytes 65568 | tf_op jit(solution)/shard_map/all_to_all | solution.py:22
  171.2 5.1 %all-to-all-start = ((bf16[32,2,2,4,128]{4,3,2,1,0:T(4,128)(2,1)}), bf16[32,2,2,4,128]{4,3,2,1,0:T(4,128)(2,1)S(1)}, u32[]{:S(2)}, u32[]{:S(2)}) async-start(bf16[32,2,2,4,128]{4,3,2,1,0:T(4,128)(2,1)} %multiply_convert_fusion.2), calls=%async_computation | async-start | bytes 262144 | tf_op jit(solution)/shard_map/all_to_all | solution.py:16
  176.4 0.2 broadcast_bitcast_fusion.1
  176.6 0.1 broadcast_bitcast_fusion
  176.6 0.0 copy-done.4
  176.6 0.6 fusion.10
  177.2 15.3 %all-to-all-done = bf16[32,2,2,4,128]{4,3,2,1,0:T(4,128)(2,1)S(1)} async-done(((bf16[32,2,2,4,128]{4,3,2,1,0:T(4,128)(2,1)}), bf16[32,2,2,4,128]{4,3,2,1,0:T(4,128)(2,1)S(1)}, u32[]{:S(2)}, u32[]{:S(2)}) %all-to-all-start) | async-done | bytes 131104 | tf_op jit(solution)/shard_map/all_to_all | solution.py:16
  192.6 0.7 reduce_sum.41
  (8 shorter events, 0.1 us)
Async XLA Ops:
  7.2 127.7 %copy-start = (bf16[4096,256]{1,0:T(8,128)(2,1)S(1)}, bf16[4096,256]{1,0:T(8,128)(2,1)}, u32[]{:S(2)}) copy-start(bf16[4096,256]{1,0:T(8,128)(2,1)} %param.10) | copy-start | bytes 6291460
  7.2 95.1 %all-gather.3.cloned.1.call-start = ((), (), s32[]{:S(2)}) async-start(), calls=%async_computation.2 | async-start | bytes 8912896 | tf_op jit(solution)/shard_map/all_gather | solution.py:54
  134.9 5.9 %copy-start.1 = (bf16[1024,4096,1]{1,0,2:T(8,128)(2,1)S(1)}, bf16[1024,4096,1]{1,0,2:T(8,128)(2,1)}, u32[]{:S(2)}) copy-start(bf16[1024,4096,1]{1,0,2:T(8,128)(2,1)} %reshape.159) | copy-start | bytes 25165828
  134.9 6.4 %copy-start.2 = (bf16[256,4096]{1,0:T(8,128)(2,1)S(1)}, bf16[256,4096]{1,0:T(8,128)(2,1)}, u32[]{:S(2)}) copy-start(bf16[256,4096]{1,0:T(8,128)(2,1)} %copy.27) | copy-start | bytes 6291460
  141.2 17.1 %copy-start.3 = (bf16[2,256]{1,0:T(2,128)(2,1)S(1)}, bf16[2,256]{1,0:T(2,128)(2,1)}, u32[]{:S(2)}) copy-start(bf16[2,256]{1,0:T(2,128)(2,1)} %param.14) | copy-start | bytes 3076
  141.2 35.4 %copy-start.4 = (f32[256]{0:T(256)S(1)}, f32[256]{0:T(256)}, u32[]{:S(2)}) copy-start(f32[256]{0:T(256)} %param.15) | copy-start | bytes 3076
  145.1 26.2 %all-to-all-start.1 = ((f32[32,2,2,128]{3,2,1,0:T(2,128)}), f32[32,2,2,128]{3,2,1,0:T(2,128)S(1)}, u32[]{:S(2)}, u32[]{:S(2)}) async-start(f32[32,2,2,128]{3,2,1,0:T(2,128)} %broadcast_in_dim.4), calls=%async_computation.1 | async-start | bytes 131072 | tf_op jit(solution)/shard_map/all_to_all | solution.py:22
  171.2 21.3 %all-to-all-start = ((bf16[32,2,2,4,128]{4,3,2,1,0:T(4,128)(2,1)}), bf16[32,2,2,4,128]{4,3,2,1,0:T(4,128)(2,1)S(1)}, u32[]{:S(2)}, u32[]{:S(2)}) async-start(bf16[32,2,2,4,128]{4,3,2,1,0:T(4,128)(2,1)} %multiply_convert_fusion.2), calls=%async_computation | async-start | bytes 262144 | tf_op jit(solution)/shard_map/all_to_all | solution.py:16
Sparse Core Ops, SparseCore 0:
  11.0 91.2 all-gather.2
